TPU v7x, 32 devices: a whole 2x2x4 slice. The times are simulated.
32 devices in a mesh: gr: 2 (over x), sp: 8 (over z, y), tp: 2 (over core).
Axes of the slice: x: 2, y: 2, z: 4, core: 2. Of those that a mesh axis runs over, the one named last changes fastest.
Arguments:
- tokens: bfloat16 [2, 2, 6144, 2048], P('gr', 'tp', 'sp'), may hold values from -6 to 6
- key_weight: bfloat16 [2048, 2048], replicated, may hold values from -0.125 to 0.125
- value_weight: bfloat16 [2048, 2048], replicated, may hold values from -0.125 to 0.125
- cum_gate: float32 [2, 32, 2, 6144], P('gr', None, 'tp', 'sp'), may hold values from -12588 to 0, as said below
- query: bfloat16 [2, 32, 64], P('gr', 'sp'), may hold values from -12 to 12
Outputs:
- kv_cache: bfloat16 [2, 32, 12288, 128], P('gr', 'sp', 'tp')
- gate_cache: float32 [2, 32, 12288], P('gr', 'sp', 'tp')
- read: bfloat16 [2, 32, 64], P('gr', 'sp')
Inputs may be any that keep to these rules, and one draw needn't show every extreme that they name: `cum_gate`: each head's entries never rise along the positions.
All inputs are finite; a program needn't handle non-finite values.
Results may differ from a plain program's by a relative error of at most 0.012.
Values may be sent and summed in bfloat16 or wider, within the bound.
A program may use at most 128 MiB of HBM per device.

v0:
```python
import jax
import jax.numpy as jnp
from jax import lax
from jax.sharding import PartitionSpec as P


def merged(value, axis, join):
    pieces = jax.tree.map(lambda part: lax.all_gather(part, axis), value)
    head = jax.tree.map(lambda part: part[0], pieces)
    tail = jax.tree.map(lambda part: part[1:], pieces)
    subtotal, _ = lax.scan(lambda subtotal, share: (join(subtotal, share), None), head, tail)
    return subtotal


def combine_reads(first, second):
    top = jnp.maximum(first[0], second[0])
    scale_one = jnp.exp(first[0] - top)
    scale_two = jnp.exp(second[0] - top)
    total = first[1] * scale_one + second[1] * scale_two
    weighted = first[2] * scale_one[..., None] + second[2] * scale_two[..., None]
    return (top, total, weighted)


def partial_read(query, keys, values, gates, head_size):
    scores = jnp.einsum("bhe,bhse->bhs", query, keys, preferred_element_type=jnp.float32)
    scores = scores * head_size ** (-0.5) - gates
    top = jnp.max(scores, axis=-1)
    weights = jnp.exp(scores - top[..., None])
    total = jnp.sum(weights, axis=-1)
    weighted = jnp.einsum(
        "bhs,bhse->bhe", weights.astype(jnp.bfloat16), values, preferred_element_type=jnp.float32
    )
    return (top, total, weighted)


def local_project(tokens, key_weight, value_weight, head_size):
    width = tokens.shape[3]
    local_rows = tokens[:, 0]
    key_part = jnp.einsum(
        "btd,dhe->bhte",
        local_rows,
        key_weight.reshape(width, -1, head_size),
        preferred_element_type=jnp.float32,
    ).astype(jnp.bfloat16)
    value_part = jnp.einsum(
        "btd,dhe->bhte",
        local_rows,
        value_weight.reshape(width, -1, head_size),
        preferred_element_type=jnp.float32,
    ).astype(jnp.bfloat16)
    return (key_part, value_part)


def on_device(tokens, key_weight, value_weight, cum_gate, query):
    count = tokens.shape[0]
    head_size = query.shape[2]
    key_part = None
    value_part = None
    key_part, value_part = local_project(tokens, key_weight, value_weight, head_size)
    joined = jnp.concatenate([key_part, value_part], axis=-1)
    kv_cache = lax.all_to_all(joined, "sp", split_axis=1, concat_axis=2, tiled=True)
    gates = lax.all_to_all(cum_gate, "sp", split_axis=1, concat_axis=3, tiled=True)
    gate_cache = gates.reshape(count, gates.shape[1], gates.shape[3])
    parts = partial_read(
        query, kv_cache[..., :head_size], kv_cache[..., head_size:], gate_cache, head_size
    )
    top, total, weighted = merged(parts, "tp", combine_reads)
    read = (weighted / total[..., None]).astype(jnp.bfloat16)
    return (kv_cache, gate_cache, read)


def solution(mesh):
    placed = (P("gr", "tp", "sp", None), P(), P(), P("gr", None, "tp", "sp"), P("gr", "sp", None))
    return jax.shard_map(
        on_device,
        mesh=mesh,
        in_specs=placed,
        out_specs=(P("gr", "sp", "tp", None), P("gr", "sp", "tp"), P("gr", "sp", None)),
        check_vma=False,
    )
```

profile of v0, /device:TPU:0, one launch (start us, length us, event | category | flops | bytes accessed | tf_op | source)
XLA Modules:
  0.0 217.3 jit_solution(17733755915182481379)
XLA Ops:
  0.6 0.0 copy-start
  0.6 7.6 %all-to-all-start.1 = ((f32[1,32,1,768]{3,2,0,1:T(1,128)}), f32[1,32,1,768]{3,2,0,1:T(1,128)S(1)}, u32[]{:S(2)}, u32[]{:S(2)}) async-start(f32[1,32,1,768]{3,2,0,1:T(1,128)} %bitcast.77), calls=%async_computation.1 | async-start | bytes 196608 | tf_op jit(solution)/shard_map/all_to_all | solution.py:62
  8.2 12.3 %copy.23 = bf16[2048,2048]{0,1:T(8,128)(2,1)} copy(bf16[2048,2048]{1,0:T(8,128)(2,1)} %param.7) | data formatting | bytes 16777216 | tf_op args[2]
  20.5 12.4 %copy.22 = bf16[2048,2048]{0,1:T(8,128)(2,1)} copy(bf16[2048,2048]{1,0:T(8,128)(2,1)} %param.6) | data formatting | bytes 16777216 | tf_op args[1]
  32.9 0.0 copy-done
  32.9 9.3 %convert_bitcast_fusion = bf16[1,32,768,64]{2,3,1,0:T(8,128)(2,1)S(1)} fusion(bf16[2048,32,64]{0,2,1:T(8,128)(2,1)} %bitcast.68, bf16[1,1,768,2048]{3,2,1,0:T(8,128)(2,1)S(1)} %copy-done), kind=kOutput, calls=%fused_computation.9 | convolution fusion | flops 6444023808 | bytes 14680064 | tf_op jit(solution)/shard_map/btd,dhe->bhte/dot_general | solution.py:45
  42.2 6.9 %convert_bitcast_fusion.1 = bf16[1,32,768,64]{2,3,1,0:T(8,128)(2,1)S(1)} fusion(bf16[2048,32,64]{0,2,1:T(8,128)(2,1)S(1)} %bitcast.67, bf16[1,1,768,2048]{3,2,1,0:T(8,128)(2,1)S(1)} %copy-done), kind=kOutput, calls=%fused_computation.10 | convolution fusion | flops 6444023808 | bytes 14680064 | tf_op jit(solution)/shard_map/btd,dhe->bhte/dot_general | solution.py:39
  49.1 3.4 %maximum_bitcast_fusion = bf16[1,32,768,128]{2,3,0,1:T(8,128)(2,1)} fusion(bf16[1,32,768,64]{2,3,1,0:T(8,128)(2,1)S(1)} %convert_bitcast_fusion, bf16[1,32,768,64]{2,3,1,0:T(8,128)(2,1)S(1)} %convert_bitcast_fusion.1), kind=kLoop, calls=%fused_computation.4 | loop fusion | flops 12582912 | bytes 12582912 | tf_op jit(solution)/shard_map/concatenate | solution.py:60
  52.5 0.0 all-to-all-done.1
  52.5 6.1 %all-to-all-start = ((bf16[1,32,768,128]{2,3,0,1:T(8,128)(2,1)}), bf16[1,32,768,128]{2,3,0,1:T(8,128)(2,1)}, u32[]{:S(2)}, u32[]{:S(2)}) async-start(bf16[1,32,768,128]{2,3,0,1:T(8,128)(2,1)} %maximum_bitcast_fusion), calls=%async_computation | async-start | bytes 12582912 | tf_op jit(solution)/shard_map/all_to_all | solution.py:61
  58.6 0.6 dynamic-slice
  59.9 0.7 reshape.234
  60.6 135.7 %all-to-all-done = bf16[1,32,768,128]{2,3,0,1:T(8,128)(2,1)} async-done(((bf16[1,32,768,128]{2,3,0,1:T(8,128)(2,1)}), bf16[1,32,768,128]{2,3,0,1:T(8,128)(2,1)}, u32[]{:S(2)}, u32[]{:S(2)}) %all-to-all-start) | async-done | bytes 6291488 | tf_op jit(solution)/shard_map/all_to_all | solution.py:61
  196.3 8.6 %copy.25 = bf16[1,4,8,768,128]{4,3,2,1,0:T(8,128)(2,1)} copy(bf16[1,4,8,768,128]{3,4,1,2,0:T(8,128)(2,1)} %bitcast.11) | data formatting | bytes 12582912 | tf_op jit(solution)/shard_map/all_to_all | solution.py:61
  204.9 4.6 %fusion.1 = f32[4,1,6144]{2,1,0:T(1,128)S(1)} fusion(bf16[1,4,6144,128]{3,2,1,0:T(8,128)(2,1)} %bitcast.69, bf16[4,64,1]{1,0,2:T(4,128)(2,1)S(1)} %bitcast.79), kind=kOutput, calls=%fused_computation.3 | convolution fusion | flops 3145728 | bytes 6390272 | tf_op jit(solution)/shard_map/bhe,bhse->bhs/dot_general | solution.py:25
  209.5 0.2 fusion.22
  209.7 0.2 fusion.12
  210.0 1.9 fusion
  211.9 0.2 dynamic-update-slice
  212.1 0.2 dynamic-update-slice.1
  212.3 1.8 all-gather.3
  214.1 2.4 %all-reduce.2 = (f32[8]{0:T(128)S(1)}, f32[8]{0:T(128)S(1)}) all-reduce(f32[8]{0:T(128)S(1)} %dynamic-update-slice, f32[8]{0:T(128)S(1)} %dynamic-update-slice.1), channel_id=3, replica_groups=mesh['gr'=2,'sp'=8,'tp'=2] {'tp'}, use_global_device_ids=true, to_apply=%add | all-reduce | flops 16 | bytes 128
  216.6 0.1 fusion.21
  216.7 0.6 fusion.18
  (12 shorter events, 0.1 us)
Async XLA Ops:
  0.6 32.2 %copy-start = (bf16[1,1,768,2048]{3,2,1,0:T(8,128)(2,1)S(1)}, bf16[1,1,768,2048]{3,2,1,0:T(8,128)(2,1)}, u32[]{:S(2)}) copy-start(bf16[1,1,768,2048]{3,2,1,0:T(8,128)(2,1)} %param.5) | copy-start | bytes 9437188
  0.6 51.8 %all-to-all-start.1 = ((f32[1,32,1,768]{3,2,0,1:T(1,128)}), f32[1,32,1,768]{3,2,0,1:T(1,128)S(1)}, u32[]{:S(2)}, u32[]{:S(2)}) async-start(f32[1,32,1,768]{3,2,0,1:T(1,128)} %bitcast.77), calls=%async_computation.1 | async-start | bytes 196608 | tf_op jit(solution)/shard_map/all_to_all | solution.py:62
  32.9 9.3 %copy-start.1 = (bf16[2048,2048]{0,1:T(8,128)(2,1)S(1)}, bf16[2048,2048]{0,1:T(8,128)(2,1)}, u32[]{:S(2)}) copy-start(bf16[2048,2048]{0,1:T(8,128)(2,1)} %copy.22) | copy-start | bytes 25165828
  52.5 6.1 %copy-start.4 = (u32[32]{0:T(128)S(1)}, u32[32]{0:T(128)}, u32[]{:S(2)}) copy-start(u32[32]{0:T(128)} %constant.21) | copy-start | bytes 388
  52.5 143.8 %all-to-all-start = ((bf16[1,32,768,128]{2,3,0,1:T(8,128)(2,1)}), bf16[1,32,768,128]{2,3,0,1:T(8,128)(2,1)}, u32[]{:S(2)}, u32[]{:S(2)}) async-start(bf16[1,32,768,128]{2,3,0,1:T(8,128)(2,1)} %maximum_bitcast_fusion), calls=%async_computation | async-start | bytes 12582912 | tf_op jit(solution)/shard_map/all_to_all | solution.py:61
  196.3 8.6 %copy-start.3 = (bf16[1,4,64]{2,1,0:T(4,128)(2,1)S(1)}, bf16[1,4,64]{2,1,0:T(4,128)(2,1)}, u32[]{:S(2)}) copy-start(bf16[1,4,64]{2,1,0:T(4,128)(2,1)} %param.9) | copy-start | bytes 1540
  204.9 5.1 %copy-start.2 = (bf16[1,4,8,768,128]{4,3,2,1,0:T(8,128)(2,1)S(1)}, bf16[1,4,8,768,128]{4,3,2,1,0:T(8,128)(2,1)}, u32[]{:S(2)}) copy-start(bf16[1,4,8,768,128]{4,3,2,1,0:T(8,128)(2,1)} %copy.25) | copy-start | bytes 18874372
where the time goes:
time: 218 us; the launch traced here: 217 us
  waiting for transfers between devices  136 us (62%)
  local copies, waits for them, and re-layouts  35 us (16%)
  matrix products  22.8 us (10%)
  starting transfers between devices  13.7 us (6%)
  other arithmetic  4.53 us (2%)
  blocking collectives  4.27 us (2%)
    all_to_all x1, waiting for transfers between devices, on_device(): lax.all_to_all(joined, 'sp', split_axis=1, concat_axis=2, tiled=True)  136 us
    unnamed x18, local copies, waits for them, and re-layouts  25.7 us
    dot_general x1, matrix products, local_project(): jnp.einsum('btd,dhe->bhte', local_rows, value_weight.reshape(width, -1, h...  9.28 us
    all_to_all x1, local copies, waits for them, and re-layouts, on_device(): lax.all_to_all(joined, 'sp', split_axis=1, concat_axis=2, tiled=True)  8.63 us
    all_to_all x1, starting transfers between devices, on_device(): lax.all_to_all(cum_gate, 'sp', split_axis=1, concat_axis=3, tiled=True)  7.58 us
    dot_general x1, matrix products, local_project(): jnp.einsum('btd,dhe->bhte', local_rows, key_weight.reshape(width, -1, hea...  6.93 us
    all_to_all x1, starting transfers between devices, on_device(): lax.all_to_all(joined, 'sp', split_axis=1, concat_axis=2, tiled=True)  6.12 us
    dot_general x1, matrix products, partial_read(): jnp.einsum('bhe,bhse->bhs', query, keys, preferred_element_type=jnp.float32)  4.64 us
  transfers between devices with their start and end apart: 2, of which 1 were waited for; matrix products, arithmetic and copies ran while one was open for 21% of the time, Pallas kernels for 0%

commit v1 on v0

--- a/solution.py
+++ b/solution.py
@@ -58,7 +58,10 @@
     value_part = None
     key_part, value_part = local_project(tokens, key_weight, value_weight, head_size)
     joined = jnp.concatenate([key_part, value_part], axis=-1)
-    kv_cache = lax.all_to_all(joined, "sp", split_axis=1, concat_axis=2, tiled=True)
+    kv_cache = jnp.concatenate(
+        lax.all_to_all(jnp.stack(jnp.split(joined, lax.axis_size("sp"), axis=1)), "sp", 0, 0),
+        axis=2,
+    )
     gates = lax.all_to_all(cum_gate, "sp", split_axis=1, concat_axis=3, tiled=True)
     gate_cache = gates.reshape(count, gates.shape[1], gates.shape[3])
     parts = partial_read(

time: 218 us -> 222 us (1.018)
  other arithmetic: 4.53 us -> 8.62 us
    all_to_all x1 -> x0, local copies, waits for them, and re-layouts: 8.63 us -> none  [on_device(): lax.all_to_all(joined, 'sp', split_axis=1, concat_axis=2, tiled=True)]
    reshape x0 -> x1, local copies, waits for them, and re-layouts: none -> 8.63 us  [on_device(): jnp.concatenate(lax.all_to_all(jnp.stack(jnp.split(joined, lax.axis_size(...]
    unnamed x0 -> x7, other arithmetic: none -> 6.52 us
    concatenate x1 -> x0, other arithmetic: 3.36 us -> none  [on_device(): joined = jnp.concatenate([key_part, value_part], axis=-1)]
  transfers between devices with their start and end apart: 2 -> 2, of which waited for: 1 -> 1; matrix products, arithmetic and copies ran while one was open for 21% -> 22% of each run, Pallas kernels for 0% -> 0%
where the time goes in v1:
time: 222 us; the launch traced here: 221 us
  waiting for transfers between devices  136 us (61%)
  local copies, waits for them, and re-layouts  35 us (16%)
  matrix products  22.8 us (10%)
  starting transfers between devices  13.7 us (6%)
  other arithmetic  8.62 us (4%)
  blocking collectives  4.27 us (2%)
    all_to_all x1, waiting for transfers between devices, on_device(): lax.all_to_all(jnp.stack(jnp.split(joined, lax.axis_size('sp'), axis=1)),...  136 us
    unnamed x18, local copies, waits for them, and re-layouts  25.7 us
    dot_general x1, matrix products, local_project(): jnp.einsum('btd,dhe->bhte', local_rows, value_weight.reshape(width, -1, h...  9.28 us
    reshape x1, local copies, waits for them, and re-layouts, on_device(): jnp.concatenate(lax.all_to_all(jnp.stack(jnp.split(joined, lax.axis_size(...  8.63 us
    all_to_all x1, starting transfers between devices, on_device(): lax.all_to_all(cum_gate, 'sp', split_axis=1, concat_axis=3, tiled=True)  7.58 us
    dot_general x1, matrix products, local_project(): jnp.einsum('btd,dhe->bhte', local_rows, key_weight.reshape(width, -1, hea...  6.93 us
    unnamed x7, other arithmetic  6.52 us
    all_to_all x1, starting transfers between devices, on_device(): lax.all_to_all(jnp.stack(jnp.split(joined, lax.axis_size('sp'), axis=1)),...  6.12 us
  transfers between devices with their start and end apart: 2, of which 1 were waited for; matrix products, arithmetic and copies ran while one was open for 22% of the time, Pallas kernels for 0%

profile of v1, /device:TPU:0, one launch (start us, length us, event | category | flops | bytes accessed | tf_op | source)
XLA Modules:
  0.0 221.4 jit_solution(11147928914449794682)
XLA Ops:
  0.6 7.6 %all-to-all-start.1 = ((f32[1,32,1,768]{3,2,0,1:T(1,128)}), f32[1,32,1,768]{3,2,0,1:T(1,128)S(1)}, u32[]{:S(2)}, u32[]{:S(2)}) async-start(f32[1,32,1,768]{3,2,0,1:T(1,128)} %bitcast.91), calls=%async_computation.1 | async-start | bytes 196608 | tf_op jit(solution)/shard_map/all_to_all | solution.py:65
  8.2 12.3 %copy.21 = bf16[2048,2048]{0,1:T(8,128)(2,1)} copy(bf16[2048,2048]{1,0:T(8,128)(2,1)} %param.7) | data formatting | bytes 16777216 | tf_op args[2]
  20.5 12.4 %copy.20 = bf16[2048,2048]{0,1:T(8,128)(2,1)} copy(bf16[2048,2048]{1,0:T(8,128)(2,1)} %param.6) | data formatting | bytes 16777216 | tf_op args[1]
  32.9 9.3 %convert_bitcast_fusion = bf16[1,32,768,64]{2,3,1,0:T(8,128)(2,1)S(1)} fusion(bf16[2048,32,64]{0,2,1:T(8,128)(2,1)} %bitcast.82, bf16[1,1,768,2048]{3,2,1,0:T(8,128)(2,1)S(1)} %copy-done), kind=kOutput, calls=%fused_computation.22 | convolution fusion | flops 6444023808 | bytes 14680064 | tf_op jit(solution)/shard_map/btd,dhe->bhte/dot_general | solution.py:45
  42.2 6.9 %convert_bitcast_fusion.1 = bf16[1,32,768,64]{2,3,1,0:T(8,128)(2,1)S(1)} fusion(bf16[2048,32,64]{0,2,1:T(8,128)(2,1)S(1)} %bitcast.81, bf16[1,1,768,2048]{3,2,1,0:T(8,128)(2,1)S(1)} %copy-done), kind=kOutput, calls=%fused_computation.23 | convolution fusion | flops 6444023808 | bytes 14680064 | tf_op jit(solution)/shard_map/btd,dhe->bhte/dot_general | solution.py:39
  49.1 0.9 bitcast_dynamic-update-slice_fusion.6
  50.0 0.9 bitcast_dynamic-update-slice_fusion.5
  51.0 0.9 bitcast_dynamic-update-slice_fusion.4
  51.9 0.9 bitcast_dynamic-update-slice_fusion.3
  52.8 0.9 bitcast_dynamic-update-slice_fusion.2
  53.8 0.9 bitcast_dynamic-update-slice_fusion.1
  54.7 0.9 bitcast_dynamic-update-slice_fusion
  55.6 0.9 fusion.18
  56.6 6.1 %all-to-all-start = ((bf16[8,1,4,768,128]{3,4,2,1,0:T(8,128)(2,1)}), bf16[8,1,4,768,128]{3,4,2,1,0:T(8,128)(2,1)}, u32[]{:S(2)}, u32[]{:S(2)}) async-start(bf16[8,1,4,768,128]{3,4,2,1,0:T(8,128)(2,1)} %fusion.18), calls=%async_computation | async-start | bytes 12582912 | tf_op jit(solution)/shard_map/all_to_all | solution.py:62
  62.7 0.6 dynamic-slice
  64.0 0.7 reshape.242
  64.7 135.7 %all-to-all-done = bf16[8,1,4,768,128]{3,4,2,1,0:T(8,128)(2,1)} async-done(((bf16[8,1,4,768,128]{3,4,2,1,0:T(8,128)(2,1)}), bf16[8,1,4,768,128]{3,4,2,1,0:T(8,128)(2,1)}, u32[]{:S(2)}, u32[]{:S(2)}) %all-to-all-start) | async-done | bytes 6291488 | tf_op jit(solution)/shard_map/all_to_all | solution.py:62
  200.3 8.6 %copy.22 = bf16[1,4,8,768,128]{4,3,2,1,0:T(8,128)(2,1)} copy(bf16[1,4,8,768,128]{3,4,1,0,2:T(8,128)(2,1)} %bitcast.17) | data formatting | bytes 12582912 | tf_op jit(solution)/shard_map/reshape | solution.py:61
  209.0 4.6 %fusion.1 = f32[4,1,6144]{2,1,0:T(1,128)S(1)} fusion(bf16[1,4,6144,128]{3,2,1,0:T(8,128)(2,1)} %bitcast.83, bf16[4,64,1]{1,0,2:T(4,128)(2,1)S(1)} %bitcast.93), kind=kOutput, calls=%fused_computation.17 | convolution fusion | flops 3145728 | bytes 6390272 | tf_op jit(solution)/shard_map/bhe,bhse->bhs/dot_general | solution.py:25
  213.8 0.2 fusion.21
  214.1 1.9 fusion
  216.4 1.8 all-gather.3
  218.2 2.4 %all-reduce.2 = (f32[8]{0:T(128)S(1)}, f32[8]{0:T(128)S(1)}) all-reduce(f32[8]{0:T(128)S(1)} %dynamic-update-slice, f32[8]{0:T(128)S(1)} %dynamic-update-slice.1), channel_id=3, replica_groups=mesh['gr'=2,'sp'=8,'tp'=2] {'tp'}, use_global_device_ids=true, to_apply=%add | all-reduce | flops 16 | bytes 128
  220.8 0.6 fusion.27
  (19 shorter events, 0.8 us)
Async XLA Ops:
  0.6 32.2 %copy-start = (bf16[1,1,768,2048]{3,2,1,0:T(8,128)(2,1)S(1)}, bf16[1,1,768,2048]{3,2,1,0:T(8,128)(2,1)}, u32[]{:S(2)}) copy-start(bf16[1,1,768,2048]{3,2,1,0:T(8,128)(2,1)} %param.5) | copy-start | bytes 9437188
  0.6 55.9 %all-to-all-start.1 = ((f32[1,32,1,768]{3,2,0,1:T(1,128)}), f32[1,32,1,768]{3,2,0,1:T(1,128)S(1)}, u32[]{:S(2)}, u32[]{:S(2)}) async-start(f32[1,32,1,768]{3,2,0,1:T(1,128)} %bitcast.91), calls=%async_computation.1 | async-start | bytes 196608 | tf_op jit(solution)/shard_map/all_to_all | solution.py:65
  32.9 9.3 %copy-start.1 = (bf16[2048,2048]{0,1:T(8,128)(2,1)S(1)}, bf16[2048,2048]{0,1:T(8,128)(2,1)}, u32[]{:S(2)}) copy-start(bf16[2048,2048]{0,1:T(8,128)(2,1)} %copy.20) | copy-start | bytes 25165828
  56.6 6.1 %copy-start.4 = (u32[32]{0:T(128)S(1)}, u32[32]{0:T(128)}, u32[]{:S(2)}) copy-start(u32[32]{0:T(128)} %constant.21) | copy-start | bytes 388
  56.6 143.8 %all-to-all-start = ((bf16[8,1,4,768,128]{3,4,2,1,0:T(8,128)(2,1)}), bf16[8,1,4,768,128]{3,4,2,1,0:T(8,128)(2,1)}, u32[]{:S(2)}, u32[]{:S(2)}) async-start(bf16[8,1,4,768,128]{3,4,2,1,0:T(8,128)(2,1)} %fusion.18), calls=%async_computation | async-start | bytes 12582912 | tf_op jit(solution)/shard_map/all_to_all | solution.py:62
  200.3 8.6 %copy-start.3 = (bf16[1,4,64]{2,1,0:T(4,128)(2,1)S(1)}, bf16[1,4,64]{2,1,0:T(4,128)(2,1)}, u32[]{:S(2)}) copy-start(bf16[1,4,64]{2,1,0:T(4,128)(2,1)} %param.9) | copy-start | bytes 1540
  209.0 5.1 %copy-start.2 = (bf16[1,4,8,768,128]{4,3,2,1,0:T(8,128)(2,1)S(1)}, bf16[1,4,8,768,128]{4,3,2,1,0:T(8,128)(2,1)}, u32[]{:S(2)}) copy-start(bf16[1,4,8,768,128]{4,3,2,1,0:T(8,128)(2,1)} %copy.22) | copy-start | bytes 18874372
